TPU v7x, 32 devices: a whole 2x2x4 slice. The times are simulated.
32 devices in a mesh: sp: 8 (over z, y), dp: 4 (over x, core).
Axes of the slice: x: 2, y: 2, z: 4, core: 2. Of those that a mesh axis runs over, the one named last changes fastest.
Arguments:
- tokens: bfloat16 [4, 2560, 2048], P('dp', 'sp'), may hold values from -6 to 6
- w_query: bfloat16 [2048, 1024], P('dp', 'sp'), may hold values from -0.125 to 0.125
- w_key: bfloat16 [2048, 1024], P('dp', 'sp'), may hold values from -0.125 to 0.125
- w_value: bfloat16 [2048, 1024], P('dp', 'sp'), may hold values from -0.125 to 0.125
- w_output: bfloat16 [1024, 2048], P('sp', 'dp'), may hold values from -0.1875 to 0.1875
- qk_gain: float32 [2, 64], replicated, may hold values from 0.4 to 7
- decay_sums: float32 [4, 16, 2560], P('dp', 'sp'), may hold values from -512 to 0, as said below
Outputs:
- layer_out: bfloat16 [4, 2560, 2048], P('dp', 'sp')
Inputs may be any that keep to these rules, and one draw needn't show every extreme that they name: `decay_sums`: each row is non-increasing along positions.
All inputs are finite; a program needn't handle non-finite values.
Results may differ from a plain program's by a relative error of at most 0.0075.
The roundings to bfloat16 on the way count: a program that leaves them out, or rounds other values in their place, can miss the bound.
Values may be sent and summed in bfloat16 or wider, within the bound.
A program may use at most 128 MiB of HBM per device.

v0:
```python
import functools

import jax
import jax.numpy as jnp
from jax import lax
from jax.experimental import pallas as pl
from jax.experimental.pallas import tpu as pltpu
from jax.sharding import PartitionSpec as P

EPS = 1e-06
DIMS_NT = (((1,), (1,)), ((), ()))


PIECES = 2
MESH = pl.DeviceIdType.MESH


def layer_kernel(
    heads, width, count, groups,
    own_ref, stacked_ref, slab_ref, gain_ref, decay_ref, out_ref,
    whole_ref, weight_ref, slabs_ref, projected_ref, key_ref, value_ref, done_ref, merged_ref,
    send_sem, recv_sem, slab_send, slab_recv, pass_send, pass_recv, weight_send, weight_recv,
    done_send, done_recv,
):
    rows, depth = own_ref.shape
    owners = 2
    block = owners * rows
    wide = heads * width
    part = rows // (2 * PIECES)
    tall = 4 if count % 4 == 0 else 1
    broad = count // tall
    me, group = lax.axis_index("sp"), lax.axis_index("dp")

    def member(spot):
        spot = lax.rem(spot + 2 * count, count)
        column, height = spot // tall, lax.rem(spot, tall)
        level = height + lax.rem(column, 2) * (tall - 1 - 2 * height)
        return level * broad + column

    level, column = me // broad, lax.rem(me, broad)
    spot = column * tall + level + lax.rem(column, 2) * (tall - 1 - 2 * level)
    ways = (1, -1)
    targets = [member(spot + way) for way in ways]
    peers = [lax.rem(group + shift, groups) for shift in range(1, groups)]

    barrier = pltpu.get_barrier_semaphore()
    for shift in range(1, count):
        other = lax.rem(me + shift, count)
        pl.semaphore_signal(barrier, inc=1, device_id={"sp": other}, device_id_type=MESH)
    for peer in peers:
        pl.semaphore_signal(barrier, inc=1, device_id={"dp": peer}, device_id_type=MESH)
    pl.semaphore_wait(barrier, count + groups - 2)

    def send(source, target, out_sem, in_sem, device):
        copy = pltpu.make_async_remote_copy(
            src_ref=source, dst_ref=target, send_sem=out_sem, recv_sem=in_sem,
            device_id=device, device_id_type=MESH,
        )
        copy.start()
        return copy

    tall_slab = slab_ref.shape[0]
    half = tall_slab // 2
    copies, passed, weights, backlog = {}, [], [], []

    def slab_place(origin, side):
        return pl.ds(pl.multiple_of(origin * tall_slab + side * half, half), half)

    def pass_on(step, side, source, place):
        for number, peer in enumerate(peers):
            passed.append(
                send(
                    source, slabs_ref.at[group, place], pass_send.at[number, step, side],
                    pass_recv.at[number, step, side], {"dp": peer},
                )
            )

    def project(place):
        projected_ref[place, :] = jnp.dot(
            whole_ref[place, :], weight_ref[...].reshape(depth, 3 * wide),
            preferred_element_type=jnp.float32,
        ).astype(jnp.bfloat16)

    for step in range(count):
        arrived = []
        for piece in range(PIECES):
            for side, way in enumerate(ways):
                offset = (side * PIECES + piece) * part
                if step:
                    copies[step - 1, piece, side].wait_recv()
                if step == count - 1:
                    continue
                origin = member(spot - way * step)
                place = pl.ds(pl.multiple_of(origin * rows + offset, part), part)
                source = own_ref.at[pl.ds(offset, part)] if step == 0 else whole_ref.at[place]
                copies[step, piece, side] = send(
                    source, whole_ref.at[place], send_sem.at[step, piece, side],
                    recv_sem.at[step, piece, side], {"sp": targets[side]},
                )
        for side, way in enumerate(ways):
            if step:
                copies[step - 1, "slab", side].wait_recv()
            origin = member(spot - way * step)
            place = slab_place(origin, side)
            source = (
                slab_ref.at[pl.ds(side * half, half)]
                if step == 0
                else slabs_ref.at[group, place]
            )
            if step < count - 1:
                copies[step, "slab", side] = send(
                    source, slabs_ref.at[group, place], slab_send.at[step, side],
                    slab_recv.at[step, side], {"sp": targets[side]},
                )
            if step == 0:
                for number, peer in enumerate(peers if side == 0 else ()):
                    weights.append(
                        send(
                            stacked_ref, weight_ref.at[group], weight_send.at[number],
                            weight_recv.at[number], {"dp": peer},
                        )
                    )
            pass_on(step, side, source, place)
            start = origin * rows + side * PIECES * part
            backlog.append(pl.ds(pl.multiple_of(start, PIECES * part), PIECES * part))
        if step == 0:
            whole_ref[pl.ds(pl.multiple_of(me * rows, rows), rows), :] = own_ref[...]
            weight_ref[group] = stacked_ref[...]
            slabs_ref[group, pl.ds(pl.multiple_of(me * tall_slab, tall_slab), tall_slab), :] = (
                slab_ref[...]
            )
        if step == min(3, count - 1):
            for copy in weights:
                copy.wait_recv()
        if step >= min(3, count - 1):
            for place in backlog:
                project(place)
            backlog = []


    def remote(source, owner):
        return pltpu.make_async_remote_copy(
            src_ref=done_ref.at[owner], dst_ref=merged_ref.at[source],
            send_sem=done_send.at[owner], recv_sem=done_recv.at[source],
            device_id={"sp": owner}, device_id_type=MESH,
        )

    def one_block(index, unused):
        place = pl.ds(pl.multiple_of(index * block, block), block)
        projected = projected_ref[place, :]

        def unit(values, gain):
            values = values.astype(jnp.float32)
            scale = lax.rsqrt(jnp.mean(values * values, axis=-1, keepdims=True) + EPS)
            return values * scale * gain

        values_turned = projected[:, 2 * wide :].astype(jnp.float32).T
        lane = lax.broadcasted_iota(jnp.int32, (block, width), 1)
        ones_lanes = jnp.where(lane < 3, 1.0, 0.0)
        sub = lax.broadcasted_iota(jnp.int32, (2 * width, block), 0)
        ones_rows = jnp.where(
            lax.broadcasted_iota(jnp.int32, (16, block), 0) == 0, 1.0, 0.0
        )
        queries = []
        for head in range(heads):
            low = head * width
            query = unit(projected[:, low : low + width], gain_ref[0:1, :]) * width ** (-0.5)
            key = unit(projected[:, wide + low : wide + low + width], gain_ref[1:2, :])
            decay = -decay_ref[head : head + 1, place]
            first = decay.astype(jnp.bfloat16).astype(jnp.float32)
            rest = decay - first
            second = rest.astype(jnp.bfloat16).astype(jnp.float32)
            third = rest - second
            parts = jnp.where(
                sub == 0, first, jnp.where(sub == 1, second, jnp.where(sub == 2, third, 0.0))
            ).T
            queries.append(jnp.concatenate([query, ones_lanes], axis=1).astype(jnp.bfloat16))
            key_ref[head, place, :] = jnp.concatenate([key, parts[:, :width]], axis=1).astype(
                jnp.bfloat16
            )
            value_ref[head, index] = jnp.concatenate(
                [values_turned[low : low + width], ones_rows], axis=0
            ).astype(jnp.bfloat16)

        def step(column, carry, masked):
            fresh = []
            for head in range(heads):
                peak, total = carry[head]
                keys = key_ref[head, pl.ds(pl.multiple_of(column * block, block), block), :]
                scores = lax.dot_general(
                    keys, queries[head], DIMS_NT, preferred_element_type=jnp.float32
                )
                if masked:
                    key_place = lax.broadcasted_iota(jnp.int32, scores.shape, 0)
                    query_place = lax.broadcasted_iota(jnp.int32, scores.shape, 1)
                    scores = jnp.where(key_place <= query_place, scores, -jnp.inf)
                higher = jnp.maximum(peak, jnp.max(scores, axis=0, keepdims=True))
                probs = jnp.exp(scores - higher).astype(jnp.bfloat16)
                total = total * jnp.exp(peak - higher) + jnp.dot(
                    value_ref[head, column], probs, preferred_element_type=jnp.float32
                )
                fresh.append((higher, total))
            return tuple(fresh)

        start = tuple(
            (
                jnp.full((1, block), -1e30, jnp.float32),
                jnp.zeros((width + 16, block), jnp.float32),
            )
            for _ in range(heads)
        )
        carry = step(index, start, True)
        carry = lax.fori_loop(0, index, lambda column, c: step(column, c, False), carry)
        outs = []
        for head in range(heads):
            total = carry[head][1]
            mixed, norm = total[:width], total[width : width + 1]
            scale = lax.rsqrt(jnp.mean(mixed * mixed, axis=0, keepdims=True) + EPS * norm * norm)
            outs.append(mixed * scale)
        turned = jnp.concatenate(outs, axis=0).T.astype(jnp.bfloat16)
        for part_index in range(owners):
            owner = index * owners + part_index
            done_ref[owner] = turned[part_index * rows : (part_index + 1) * rows]

            @pl.when(owner != me)
            def _():
                remote(me, owner).start()

        return unused

    lax.fori_loop(0, count // owners, one_block, 0)
    merged_ref[me] = done_ref[me]
    for copy in passed:
        copy.wait_recv()
    for shift in range(1, count):
        other = lax.rem(me + shift, count)
        remote(other, other).wait_recv()
    merged = jnp.concatenate([merged_ref[source] for source in range(count)], axis=1)
    columns = slab_ref.shape[1]
    for place in range(groups):
        out_ref[:, place * columns : (place + 1) * columns] = jnp.dot(
            merged, slabs_ref[place], preferred_element_type=jnp.float32
        ).astype(out_ref.dtype)
    for copy in (*copies.values(), *passed, *weights):
        copy.wait_send()
    for shift in range(1, count):
        remote(me, lax.rem(me + shift, count)).wait_send()


def on_device(tokens, w_query, w_key, w_value, w_output, qk_gain, decay_sums):
    own_rows, decay_rows = tokens[0], decay_sums[0]
    count, groups = lax.axis_size("sp"), lax.axis_size("dp")
    rows, depth = own_rows.shape
    heads, width = decay_rows.shape[0], qk_gain.shape[1]
    wide, length, block = heads * width, count * rows, 2 * rows
    stacked = jnp.concatenate((w_query, w_key, w_value), axis=1)
    tall_slab, columns = w_output.shape
    bf16, sem = jnp.bfloat16, pltpu.SemaphoreType.DMA
    ring = (count - 1, PIECES, 2)
    result = pl.pallas_call(
        functools.partial(layer_kernel, heads, width, count, groups),
        out_shape=jax.ShapeDtypeStruct((rows, depth), bf16),
        in_specs=[pl.BlockSpec(memory_space=pltpu.VMEM)] * 5,
        out_specs=pl.BlockSpec(memory_space=pltpu.VMEM),
        scratch_shapes=[
            pltpu.VMEM((length, depth), bf16),
            pltpu.VMEM((groups, depth // groups, 3 * wide), bf16),
            pltpu.VMEM((groups, count * tall_slab, columns), bf16),
            pltpu.VMEM((length, 3 * wide), bf16),
            pltpu.VMEM((heads, length, 2 * width), bf16),
            pltpu.VMEM((heads, length // block, width + 16, block), bf16),
            pltpu.VMEM((count, rows, wide), bf16),
            pltpu.VMEM((count, rows, wide), bf16),
            sem(ring), sem(ring), sem((count - 1, 2)), sem((count - 1, 2)),
            sem((groups - 1, count, 2)), sem((groups - 1, count, 2)),
            sem((groups - 1,)), sem((groups - 1,)), sem((count,)), sem((count,)),
        ],
        compiler_params=pltpu.CompilerParams(
            collective_id=0, has_side_effects=True, vmem_limit_bytes=60 * 1024 * 1024
        ),
    )(own_rows, stacked, w_output, qk_gain, decay_rows)
    return result[None]


def solution(mesh):
    placed = (
        P("dp", "sp", None),
        P("dp", "sp"),
        P("dp", "sp"),
        P("dp", "sp"),
        P("sp", "dp"),
        P(),
        P("dp", "sp", None),
    )
    return jax.shard_map(
        on_device, mesh=mesh, in_specs=placed, out_specs=P("dp", "sp", None), check_vma=False
    )
```

profile of v0, /device:TPU:29, one launch (start us, length us, event | category | flops | bytes accessed | tf_op | source)
XLA Modules:
  0.0 156.2 jit_solution(12618242088514425663)
XLA Ops:
  0.0 1.8 %pad_maximum_fusion.stacked_ref = bf16[512,384]{1,0:T(8,128)(2,1)} fusion(bf16[512,128]{1,0:T(8,128)(2,1)} %param.10, bf16[512,128]{1,0:T(8,128)(2,1)} %param.9, bf16[512,128]{1,0:T(8,128)(2,1)} %param.8), kind=kLoop, calls=%fused_computation | loop fusion | flops 1179648 | bytes 786432 | tf_op jit(solution)/shard_map/concatenate | solution.py:256
  1.8 151.8 %shard_map.73 = bf16[320,2048]{1,0:T(8,128)(2,1)} custom-call(bf16[320,2048]{1,0:T(8,128)(2,1)} %bitcast.4, bf16[512,384]{1,0:T(8,128)(2,1)} %pad_maximum_fusion.stacked_ref, bf16[128,512]{1,0:T(8,128)(2,1)} %slab_ref.1, f32[2,64]{1,0:T(2,128)} %gain_ref.1, f32[2,2560]{1,0:T(2,128)} %bitcast.5), custom_call_target="tpu_custom_call" | custom-call | tf_op jit(solution)/shard_map/pallas_call | solution.py:260
  153.6 2.5 %copy.9 = bf16[1,320,2048]{2,1,0:T(8,128)(2,1)} copy(bf16[1,320,2048]{2,1,0:T(8,128)(2,1)} %bitcast.3) | data formatting | bytes 2621440
where the time goes:
time: 156 us
  Pallas kernels  152 us (97%)
  local copies, waits for them, and re-layouts  2.52 us (2%)
  other arithmetic  1.83 us (1%)
    pallas_call x1, Pallas kernels, on_device(): pl.pallas_call(functools.partial(layer_kernel, heads, width, count, group...  152 us

commit v1 on v0

v1 whole, which is shorter than its diff:
```python
import functools

import jax
import jax.numpy as jnp
from jax import lax
from jax.experimental import pallas as pl
from jax.experimental.pallas import tpu as pltpu
from jax.sharding import PartitionSpec as P

EPS = 1e-06
DIMS_NT = (((1,), (1,)), ((), ()))
MESH = pl.DeviceIdType.MESH
CORES = 2


def layout(count, groups):
    tall = 4 if count % 4 == 0 else 1
    return tall, count // tall, groups // CORES


def layer_kernel(
    heads, width, count, groups,
    own_ref, wq_ref, wk_ref, wv_ref, slab_ref, gain_ref, decay_ref, out_ref,
    far_ref, unit_weight_ref, value_weight_ref, slabs_ref, unit_stage_ref, value_stage_ref,
    unit_ref, val_ref, key_ref, value_ref, done_ref, merged_ref,
    far_send, far_recv, wz_send, wx_send, wc_send, w_recv, move_send, move_recv,
    sz_send, sz_recv, sy_send, sy_recv, sx_send, sx_recv, sc_send, sc_recv, done_send, done_recv,
):
    rows, depth = own_ref.shape
    part = wq_ref.shape[0]
    owners = 2
    block = owners * rows
    wide = heads * width
    tall, broad, across = layout(count, groups)
    me, group = lax.axis_index("sp"), lax.axis_index("dp")
    z, y = me // broad, lax.rem(me, broad)
    x, core = group // CORES, lax.rem(group, CORES)
    partner = x * CORES + 1 - core

    def plane(shift):
        return lax.rem(z + shift, tall)

    def along_x(shift):
        return lax.rem(x + shift, across)

    def along_y(shift):
        return lax.rem(y + shift, broad)

    barrier = pltpu.get_barrier_semaphore()
    for shift in range(1, count):
        other = lax.rem(me + shift, count)
        pl.semaphore_signal(barrier, inc=1, device_id={"sp": other}, device_id_type=MESH)
    for shift in range(1, groups):
        peer = lax.rem(group + shift, groups)
        pl.semaphore_signal(barrier, inc=1, device_id={"dp": peer}, device_id_type=MESH)
    pl.semaphore_wait(barrier, count + groups - 2)

    def remote(source, target, out_sem, in_sem, device):
        return pltpu.make_async_remote_copy(
            src_ref=source, dst_ref=target, send_sem=out_sem, recv_sem=in_sem,
            device_id=device, device_id_type=MESH,
        )

    tokens = [
        remote(
            own_ref, far_ref.at[broad - shift - 1], far_send.at[shift - 1],
            far_recv.at[broad - shift - 1], {"sp": z * broad + along_y(shift)},
        )
        for shift in range(1, broad)
    ]

    chunks = [("unit", 0), ("value", 0)] + [("unit", head) for head in range(1, heads)]
    weights = [
        unit_weight_ref.at[head] if kind == "unit" else value_weight_ref for kind, head in chunks
    ]

    def weight(number, level, owner, out_sem, device):
        piece = weights[number].at[level, owner]
        return remote(piece, piece, out_sem, w_recv.at[number, level, owner], device)

    def up(number, level):
        return weight(
            number, level, group, wz_send.at[number, level, 0], {"sp": (z + 1) * broad + y}
        )

    def down(number, level):
        return weight(
            number, level, group, wz_send.at[number, level, 1], {"sp": (z - 1) * broad + y}
        )

    def sideways(number, level):
        return [
            weight(
                number, level, group, wx_send.at[number, level, shift - 1],
                {"dp": along_x(shift) * CORES + core},
            )
            for shift in range(1, across)
        ]

    def to_core(number, level, column):
        return weight(
            number, level, column * CORES + core, wc_send.at[number, level, column],
            {"dp": partner},
        )

    def own_weight(number):
        @pl.when(z + 1 < tall)
        def _():
            up(number, z).start()

        @pl.when(z > 0)
        def _():
            down(number, z).start()

        for copy in sideways(number, z):
            copy.start()
        to_core(number, z, x).start()

    def relay(number, distance):
        @pl.when(z - distance >= 0)
        def _():
            level = z - distance
            up(number, level).wait_recv()

            @pl.when(z + 1 < tall)
            def _():
                up(number, level).start()

            for copy in sideways(number, level):
                copy.start()
            to_core(number, level, x).start()

        @pl.when(z + distance < tall)
        def _():
            level = z + distance
            down(number, level).wait_recv()

            @pl.when(z > 0)
            def _():
                down(number, level).start()

            for copy in sideways(number, level):
                copy.start()
            to_core(number, level, x).start()

    def relay_core(number):
        for turn in range(tall):
            for shift in range(1, across):
                level, column = plane(turn), along_x(shift)
                copy = to_core(number, level, column)
                weight(
                    number, level, column * CORES + core, wc_send.at[number, level, column],
                    {"dp": partner},
                ).wait_recv()
                copy.start()

    def gathered(number):
        for turn in range(tall):
            for column in range(across):
                level = plane(turn)
                weight(
                    number, level, column * CORES + 1 - core, wc_send.at[number, level, column],
                    {"dp": partner},
                ).wait_recv()

    def weights_sent(number):
        for turn in range(tall):
            level = plane(turn)

            @pl.when((level <= z) & (z + 1 < tall))
            def _():
                up(number, level).wait_send()

            @pl.when((level >= z) & (z > 0))
            def _():
                down(number, level).wait_send()

            for copy in sideways(number, level):
                copy.wait_send()
            for column in range(across):
                to_core(number, level, column).wait_send()

    lane = lax.broadcasted_iota(jnp.int32, (rows, 2 * width), 1)
    gain = jnp.concatenate([gain_ref[0:1, :] * width ** (-0.5), gain_ref[1:2, :]], axis=1)

    def unit(values):
        values = values.astype(jnp.bfloat16).astype(jnp.float32)
        squares = values * values
        first = jnp.sum(jnp.where(lane < width, squares, 0.0), axis=-1, keepdims=True)
        second = jnp.sum(jnp.where(lane < width, 0.0, squares), axis=-1, keepdims=True)
        scale = jnp.where(
            lane < width, lax.rsqrt(first / width + EPS), lax.rsqrt(second / width + EPS)
        )
        return values * scale * gain

    def move(number, turn, side):
        kind, head = chunks[number]
        source = z * broad + along_y(side)
        place = pl.ds(pl.multiple_of(source * rows, rows), rows)
        if kind == "unit":
            staged, target = unit_stage_ref.at[head, side, turn], unit_ref.at[head, place]
        else:
            staged, target = value_stage_ref.at[side, turn], val_ref.at[place]
        return remote(
            staged, target, move_send.at[number, side, turn], move_recv.at[number, source],
            {"sp": plane(turn) * broad + y},
        )

    turns = sorted(range(tall), key=lambda turn: (turn == 0, turn != tall // 2))

    def project(number, side):
        kind, head = chunks[number]
        values = own_ref[...] if side == 0 else far_ref[side - 1]
        lanes = weights[number].shape[-1]
        bunch = 2 if lanes % 128 == 0 and tall % 2 == 0 else 1
        for first in range(0, tall, bunch):
            some = turns[first : first + bunch]
            columns = [
                weights[number][plane(turn)].reshape(depth, lanes) for turn in some
            ]
            result = jnp.dot(
                values, columns[0] if bunch == 1 else jnp.concatenate(columns, axis=1),
                preferred_element_type=jnp.float32,
            )
            for index, turn in enumerate(some):
                piece = result[:, index * lanes : (index + 1) * lanes]
                piece = (unit(piece) if kind == "unit" else piece).astype(jnp.bfloat16)
                if turn:
                    if kind == "unit":
                        unit_stage_ref[head, side, turn] = piece
                    else:
                        value_stage_ref[side, turn] = piece
                    move(number, turn, side).start()
                else:
                    place = (z * broad + along_y(side)) * rows
                    place = pl.ds(pl.multiple_of(place, rows), rows)
                    if kind == "unit":
                        unit_ref[head, place, :] = piece
                    else:
                        val_ref[place, :] = piece

    def moved(number):
        kind, head = chunks[number]
        for turn in range(1, tall):
            for column in range(broad):
                source = plane(turn) * broad + column
                place = pl.ds(pl.multiple_of(source * rows, rows), rows)
                target = unit_ref.at[head, place] if kind == "unit" else val_ref.at[place]
                remote(
                    target, target, move_send.at[number, 0, turn], move_recv.at[number, source],
                    {"sp": source},
                ).wait_recv()

    tall_slab = slab_ref.shape[0]

    def slab_z(level, way):
        place = pl.ds(pl.multiple_of(level * tall_slab, tall_slab), tall_slab)
        piece = slabs_ref.at[group, y, place]
        return remote(
            piece, piece, sz_send.at[level, way], sz_recv.at[level],
            {"sp": (z + 1 - 2 * way) * broad + y},
        )

    def slab_relay(distance):
        for way in range(2):
            level = z - distance if way == 0 else z + distance
            inside = (level >= 0) if way == 0 else (level < tall)
            onward = (z + 1 < tall) if way == 0 else (z > 0)
            if distance:
                @pl.when(inside)
                def _():
                    slab_z(level, way).wait_recv()

            @pl.when(inside & onward)
            def _():
                slab_z(level, way).start()

    def slab_y(shift):
        piece = slabs_ref.at[group, y]
        return remote(
            piece, piece, sy_send.at[shift - 1], sy_recv.at[y],
            {"sp": z * broad + along_y(shift)},
        )

    def slab_x(column, shift):
        piece = slabs_ref.at[group, column]
        return remote(
            piece, piece, sx_send.at[column, shift - 1], sx_recv.at[x, column],
            {"dp": along_x(shift) * CORES + core},
        )

    def slab_core(level, column):
        piece = slabs_ref.at[level * CORES + core, column]
        return remote(
            piece, piece, sc_send.at[level, column], sc_recv.at[level, column], {"dp": partner}
        )

    def slab_spread(column):
        for shift in range(1, across):
            slab_x(column, shift).start()
        slab_core(x, column).start()

    def slabs_of_y():
        for shift in range(1, broad):
            slab_y(shift).start()
        slab_spread(y)

    def slabs_from_y():
        for shift in range(1, broad):
            column = along_y(shift)
            piece = slabs_ref.at[group, column]
            remote(
                piece, piece, sy_send.at[shift - 1], sy_recv.at[column], {"sp": me}
            ).wait_recv()
            slab_spread(column)

    def slabs_from_x():
        for turn in range(broad):
            column = along_y(turn)
            for shift in range(1, across):
                level = along_x(shift)
                piece = slabs_ref.at[level * CORES + core, column]
                remote(
                    piece, piece, sx_send.at[column, shift - 1], sx_recv.at[level, column],
                    {"dp": group},
                ).wait_recv()
                slab_core(level, column).start()

    def slabs_from_core():
        for level in range(across):
            for column in range(broad):
                piece = slabs_ref.at[level * CORES + 1 - core, column]
                remote(
                    piece, piece, sc_send.at[level, column], sc_recv.at[level, column],
                    {"dp": partner},
                ).wait_recv()

    for number, (kind, head) in enumerate(chunks):
        if kind == "unit":
            low = head * width
            pair = [ref[:, low : low + width].astype(jnp.float32) for ref in (wq_ref, wk_ref)]
            unit_weight_ref[head, z, group] = jnp.concatenate(pair, axis=1).astype(jnp.bfloat16)
        else:
            value_weight_ref[z, group] = wv_ref[...]
        own_weight(number)
        if number == 0:
            for copy in tokens:
                copy.start()
    slabs_ref[group, y, pl.ds(pl.multiple_of(z * tall_slab, tall_slab), tall_slab), :] = slab_ref[
        ...
    ]

    def relays(number):
        for distance in range(1, tall):
            relay(number, distance)

    def ready(number):
        relay_core(number)
        gathered(number)

    last = len(chunks) - 1
    relays(0)
    ready(0)
    for number in range(1, len(chunks)):
        relays(number)
        project(number - 1, 0)
        ready(number)
    for number in range(last):
        if number == 0:
            for copy in tokens:
                copy.wait_recv()
        for side in range(1, broad):
            project(number, side)
    slab_relay(0)
    for side in range(broad):
        project(last, side)
    for distance in range(1, tall):
        slab_relay(distance)
    slabs_of_y()
    for number in range(len(chunks)):
        moved(number)

    def remote_done(source, owner):
        return remote(
            done_ref.at[owner], merged_ref.at[source], done_send.at[owner], done_recv.at[source],
            {"sp": owner},
        )

    def one_block(index, unused):
        place = pl.ds(pl.multiple_of(index * block, block), block)
        values_turned = val_ref[place, :].astype(jnp.float32).T
        lane = lax.broadcasted_iota(jnp.int32, (block, 2 * width), 1)
        ones_lanes = jnp.where(lane < 3, 1.0, 0.0)
        sub = lax.broadcasted_iota(jnp.int32, (2 * width, block), 0)
        ones_rows = jnp.where(
            lax.broadcasted_iota(jnp.int32, (16, block), 0) == 0, 1.0, 0.0
        )
        queries = []
        for head in range(heads):
            low = head * width
            units = unit_ref[head, place, :].astype(jnp.float32)
            decay = -decay_ref[head : head + 1, place]
            first = decay.astype(jnp.bfloat16).astype(jnp.float32)
            rest = decay - first
            second = rest.astype(jnp.bfloat16).astype(jnp.float32)
            third = rest - second
            parts = jnp.where(
                sub == 0, first, jnp.where(sub == 1, second, jnp.where(sub == 2, third, 0.0))
            ).T
            turned_units = pltpu.roll(units, width, 1)
            queries.append(jnp.where(lane < width, ones_lanes, turned_units).astype(jnp.bfloat16))
            key_ref[head, place, :] = jnp.where(lane < width, parts, units).astype(jnp.bfloat16)
            value_ref[head, index] = jnp.concatenate(
                [values_turned[low : low + width], ones_rows], axis=0
            ).astype(jnp.bfloat16)

        def step(column, carry, masked):
            fresh = []
            for head in range(heads):
                peak, total = carry[head]
                keys = key_ref[head, pl.ds(pl.multiple_of(column * block, block), block), :]
                scores = lax.dot_general(
                    keys, queries[head], DIMS_NT, preferred_element_type=jnp.float32
                )
                if masked:
                    key_place = lax.broadcasted_iota(jnp.int32, scores.shape, 0)
                    query_place = lax.broadcasted_iota(jnp.int32, scores.shape, 1)
                    scores = jnp.where(key_place <= query_place, scores, -jnp.inf)
                higher = jnp.maximum(peak, jnp.max(scores, axis=0, keepdims=True))
                probs = jnp.exp(scores - higher).astype(jnp.bfloat16)
                total = total * jnp.exp(peak - higher) + jnp.dot(
                    value_ref[head, column], probs, preferred_element_type=jnp.float32
                )
                fresh.append((higher, total))
            return tuple(fresh)

        start = tuple(
            (
                jnp.full((1, block), -1e30, jnp.float32),
                jnp.zeros((width + 16, block), jnp.float32),
            )
            for _ in range(heads)
        )
        carry = step(index, start, True)
        carry = lax.fori_loop(0, index, lambda column, c: step(column, c, False), carry)
        outs = []
        for head in range(heads):
            total = carry[head][1]
            mixed, norm = total[:width], total[width : width + 1]
            scale = lax.rsqrt(jnp.mean(mixed * mixed, axis=0, keepdims=True) + EPS * norm * norm)
            outs.append(mixed * scale)
        turned = jnp.concatenate(outs, axis=0).T.astype(jnp.bfloat16)
        for part_index in range(owners):
            owner = index * owners + part_index
            done_ref[owner] = turned[part_index * rows : (part_index + 1) * rows]

            @pl.when(owner != me)
            def _():
                remote_done(me, owner).start()

        @pl.when(index == 1)
        def _():
            slabs_from_y()

        @pl.when(index == 2)
        def _():
            slabs_from_x()

        return unused

    lax.fori_loop(0, count // owners, one_block, 0)
    merged_ref[me] = done_ref[me]
    slabs_from_core()
    for shift in range(1, count):
        other = lax.rem(me + shift, count)
        remote_done(other, other).wait_recv()
    merged = jnp.concatenate(
        [merged_ref[level * broad + column] for column in range(broad) for level in range(tall)],
        axis=1,
    )
    columns = slab_ref.shape[1]
    for place in range(groups):
        out_ref[:, place * columns : (place + 1) * columns] = jnp.dot(
            merged, slabs_ref[place].reshape(-1, columns), preferred_element_type=jnp.float32
        ).astype(out_ref.dtype)

    for copy in tokens:
        copy.wait_send()
    for number in range(len(chunks)):
        weights_sent(number)
        for side in range(broad):
            for turn in range(1, tall):
                move(number, turn, side).wait_send()
    for distance in range(tall):
        for way in range(2):
            level = z - distance if way == 0 else z + distance
            inside = (level >= 0) if way == 0 else (level < tall)
            onward = (z + 1 < tall) if way == 0 else (z > 0)

            @pl.when(inside & onward)
            def _():
                slab_z(level, way).wait_send()

    for shift in range(1, broad):
        slab_y(shift).wait_send()
    for column in range(broad):
        for shift in range(1, across):
            slab_x(column, shift).wait_send()
        for level in range(across):
            slab_core(level, column).wait_send()
    for shift in range(1, count):
        remote_done(me, lax.rem(me + shift, count)).wait_send()


def on_device(tokens, w_query, w_key, w_value, w_output, qk_gain, decay_sums):
    own_rows, decay_rows = tokens[0], decay_sums[0]
    count, groups = lax.axis_size("sp"), lax.axis_size("dp")
    tall, broad, across = layout(count, groups)
    rows, depth = own_rows.shape
    part = w_query.shape[0]
    heads, width = decay_rows.shape[0], qk_gain.shape[1]
    wide, length, block = heads * width, count * rows, 2 * rows
    tall_slab, columns = w_output.shape
    bf16, sem, chunks = jnp.bfloat16, pltpu.SemaphoreType.DMA, heads + 1
    others, beside = max(broad - 1, 1), max(across - 1, 1)
    result = pl.pallas_call(
        functools.partial(layer_kernel, heads, width, count, groups),
        out_shape=jax.ShapeDtypeStruct((rows, depth), bf16),
        in_specs=[pl.BlockSpec(memory_space=pltpu.VMEM)] * 7,
        out_specs=pl.BlockSpec(memory_space=pltpu.VMEM),
        scratch_shapes=[
            pltpu.VMEM((others, rows, depth), bf16),
            pltpu.VMEM((heads, tall, groups, part, 2 * width), bf16),
            pltpu.VMEM((tall, groups, part, wide), bf16),
            pltpu.VMEM((groups, broad, tall * tall_slab, columns), bf16),
            pltpu.VMEM((heads, broad, tall, rows, 2 * width), bf16),
            pltpu.VMEM((broad, tall, rows, wide), bf16),
            pltpu.VMEM((heads, length, 2 * width), bf16),
            pltpu.VMEM((length, wide), bf16),
            pltpu.VMEM((heads, length, 2 * width), bf16),
            pltpu.VMEM((heads, length // block, width + 16, block), bf16),
            pltpu.VMEM((count, rows, wide), bf16),
            pltpu.VMEM((count, rows, wide), bf16),
            sem((others,)), sem((others,)),
            sem((chunks, tall, 2)), sem((chunks, tall, beside)), sem((chunks, tall, across)),
            sem((chunks, tall, groups)),
            sem((chunks, broad, tall)), sem((chunks, count)),
            sem((tall, 2)), sem((tall,)), sem((others,)), sem((broad,)),
            sem((broad, beside)), sem((across, broad)), sem((across, broad)), sem((across, broad)),
            sem((count,)), sem((count,)),
        ],
        compiler_params=pltpu.CompilerParams(
            collective_id=0, has_side_effects=True, vmem_limit_bytes=60 * 1024 * 1024
        ),
    )(own_rows, w_query, w_key, w_value, w_output, qk_gain, decay_rows)
    return result[None]


def solution(mesh):
    placed = (
        P("dp", "sp", None),
        P("dp", "sp"),
        P("dp", "sp"),
        P("dp", "sp"),
        P("sp", "dp"),
        P(),
        P("dp", "sp", None),
    )
    return jax.shard_map(
        on_device, mesh=mesh, in_specs=placed, out_specs=P("dp", "sp", None), check_vma=False
    )
```

time: 156 us -> 139 us (0.89)
  the two profiles are of different devices: /device:TPU:29 before, /device:TPU:26 now
where the time goes in v1:
time: 139 us
  Pallas kernels  136 us (98%)
  local copies, waits for them, and re-layouts  2.52 us (2%)
    pallas_call x1, Pallas kernels, on_device(): pl.pallas_call(functools.partial(layer_kernel, heads, width, count, group...  136 us

profile of v1, /device:TPU:26, one launch (start us, length us, event | category | flops | bytes accessed | tf_op | source)
XLA Modules:
  0.0 138.5 jit_solution(13176956515751673859)
XLA Ops:
  0.0 136.0 %shard_map.73 = bf16[320,2048]{1,0:T(8,128)(2,1)} custom-call(bf16[320,2048]{1,0:T(8,128)(2,1)} %bitcast.4, bf16[512,128]{1,0:T(8,128)(2,1)} %wq_ref.1, bf16[512,128]{1,0:T(8,128)(2,1)} %wk_ref.1, bf16[512,128]{1,0:T(8,128)(2,1)} %wv_ref.1, bf16[128,512]{1,0:T(8,128)(2,1)} %slab_ref.1, f32[2,64]{1,0:T(2,128)} %gain_ref.1, f32[2,2560]{1,0:T(2,128)} %bitcast.5), custom_call_target="tpu_custom_call" | custom-call | tf_op jit(solution)/shard_map/pallas_call | solution.py:526
  136.0 2.5 %copy.9 = bf16[1,320,2048]{2,1,0:T(8,128)(2,1)} copy(bf16[1,320,2048]{2,1,0:T(8,128)(2,1)} %bitcast.3) | data formatting | bytes 2621440

commit v2 on v1

--- a/solution.py
+++ b/solution.py
@@ -103,7 +103,7 @@
             {"dp": partner},
         )
 
-    def own_weight(number):
+    def own_along_z(number):
         @pl.when(z + 1 < tall)
         def _():
             up(number, z).start()
@@ -112,36 +112,28 @@
         def _():
             down(number, z).start()
 
-        for copy in sideways(number, z):
+    def spread(number, level):
+        for copy in sideways(number, level):
             copy.start()
-        to_core(number, z, x).start()
-
-    def relay(number, distance):
-        @pl.when(z - distance >= 0)
-        def _():
-            level = z - distance
-            up(number, level).wait_recv()
-
-            @pl.when(z + 1 < tall)
+        to_core(number, level, x).start()
+
+    def relay(number, distance, onward=True, across_too=True):
+        for way, step in enumerate((up, down)):
+            level = z - distance if way == 0 else z + distance
+            inside = (level >= 0) if way == 0 else (level < tall)
+            more = (z + 1 < tall) if way == 0 else (z > 0)
+
+            @pl.when(inside)
             def _():
-                up(number, level).start()
-
-            for copy in sideways(number, level):
-                copy.start()
-            to_core(number, level, x).start()
-
-        @pl.when(z + distance < tall)
-        def _():
-            level = z + distance
-            down(number, level).wait_recv()
-
-            @pl.when(z > 0)
-            def _():
-                down(number, level).start()
-
-            for copy in sideways(number, level):
-                copy.start()
-            to_core(number, level, x).start()
+                if onward:
+                    step(number, level).wait_recv()
+
+                    @pl.when(more)
+                    def _():
+                        step(number, level).start()
+
+                if across_too:
+                    spread(number, level)
 
     def relay_core(number):
         for turn in range(tall):
@@ -275,18 +267,18 @@
             def _():
                 slab_z(level, way).start()
 
-    def slab_y(shift):
+    def slab_x(shift):
         piece = slabs_ref.at[group, y]
         return remote(
-            piece, piece, sy_send.at[shift - 1], sy_recv.at[y],
+            piece, piece, sx_send.at[shift - 1], sx_recv.at[x],
+            {"dp": along_x(shift) * CORES + core},
+        )
+
+    def slab_y(level, shift):
+        piece = slabs_ref.at[level * CORES + core, y]
+        return remote(
+            piece, piece, sy_send.at[level, shift - 1], sy_recv.at[level, y],
             {"sp": z * broad + along_y(shift)},
-        )
-
-    def slab_x(column, shift):
-        piece = slabs_ref.at[group, column]
-        return remote(
-            piece, piece, sx_send.at[column, shift - 1], sx_recv.at[x, column],
-            {"dp": along_x(shift) * CORES + core},
         )
 
     def slab_core(level, column):
@@ -295,34 +287,34 @@
             piece, piece, sc_send.at[level, column], sc_recv.at[level, column], {"dp": partner}
         )
 
-    def slab_spread(column):
+    def slab_spread(level):
+        for shift in range(1, broad):
+            slab_y(level, shift).start()
+        slab_core(level, y).start()
+
+    def slabs_of_y():
         for shift in range(1, across):
-            slab_x(column, shift).start()
-        slab_core(x, column).start()
-
-    def slabs_of_y():
-        for shift in range(1, broad):
-            slab_y(shift).start()
-        slab_spread(y)
+            slab_x(shift).start()
+        slab_spread(x)
+
+    def slabs_from_x():
+        for shift in range(1, across):
+            level = along_x(shift)
+            piece = slabs_ref.at[level * CORES + core, y]
+            remote(
+                piece, piece, sx_send.at[shift - 1], sx_recv.at[level], {"dp": group}
+            ).wait_recv()
+            slab_spread(level)
 
     def slabs_from_y():
-        for shift in range(1, broad):
-            column = along_y(shift)
-            piece = slabs_ref.at[group, column]
-            remote(
-                piece, piece, sy_send.at[shift - 1], sy_recv.at[column], {"sp": me}
-            ).wait_recv()
-            slab_spread(column)
-
-    def slabs_from_x():
-        for turn in range(broad):
-            column = along_y(turn)
-            for shift in range(1, across):
-                level = along_x(shift)
+        for turn in range(across):
+            level = along_x(turn)
+            for shift in range(1, broad):
+                column = along_y(shift)
                 piece = slabs_ref.at[level * CORES + core, column]
                 remote(
-                    piece, piece, sx_send.at[column, shift - 1], sx_recv.at[level, column],
-                    {"dp": group},
+                    piece, piece, sy_send.at[level, shift - 1], sy_recv.at[level, column],
+                    {"sp": me},
                 ).wait_recv()
                 slab_core(level, column).start()
 
@@ -342,7 +334,9 @@
             unit_weight_ref[head, z, group] = jnp.concatenate(pair, axis=1).astype(jnp.bfloat16)
         else:
             value_weight_ref[z, group] = wv_ref[...]
-        own_weight(number)
+        if number < 2:
+            own_along_z(number)
+            spread(number, z)
         if number == 0:
             for copy in tokens:
                 copy.start()
@@ -350,33 +344,52 @@
         ...
     ]
 
-    def relays(number):
-        for distance in range(1, tall):
-            relay(number, distance)
-
     def ready(number):
         relay_core(number)
         gathered(number)
 
     last = len(chunks) - 1
-    relays(0)
+    rest = range(2, len(chunks))
+    for distance in range(1, tall):
+        relay(0, distance)
+        if distance == 1:
+            relay(1, 1, across_too=False)
+            for number in rest:
+                own_along_z(number)
+        elif distance == 2:
+            relay(1, 1, onward=False)
+            relay(1, 2, across_too=False)
+    for number in rest:
+        relay(number, 1, across_too=False)
+    if tall > 2:
+        relay(1, 2, onward=False)
     ready(0)
-    for number in range(1, len(chunks)):
-        relays(number)
-        project(number - 1, 0)
-        ready(number)
-    for number in range(last):
-        if number == 0:
-            for copy in tokens:
-                copy.wait_recv()
+    for distance in range(3, tall):
+        relay(1, distance)
+    project(0, 0)
+    for number in rest:
+        spread(number, z)
+        relay(number, 1, onward=False)
+        if tall > 2:
+            relay(number, 2)
+    ready(1)
+    for number in rest:
+        for distance in range(3, tall):
+            relay(number, distance)
+    project(1, 0)
+    slab_relay(0)
+    for copy in tokens:
+        copy.wait_recv()
+    for number in range(2):
         for side in range(1, broad):
             project(number, side)
-    slab_relay(0)
-    for side in range(broad):
-        project(last, side)
     for distance in range(1, tall):
         slab_relay(distance)
     slabs_of_y()
+    for number in rest:
+        ready(number)
+        for side in range(broad):
+            project(number, side)
     for number in range(len(chunks)):
         moved(number)
 
@@ -460,11 +473,11 @@
 
         @pl.when(index == 1)
         def _():
+            slabs_from_x()
+
+        @pl.when(index == 3)
+        def _():
             slabs_from_y()
-
-        @pl.when(index == 2)
-        def _():
-            slabs_from_x()
 
         return unused
 
@@ -501,12 +514,12 @@
             def _():
                 slab_z(level, way).wait_send()
 
-    for shift in range(1, broad):
-        slab_y(shift).wait_send()
-    for column in range(broad):
-        for shift in range(1, across):
-            slab_x(column, shift).wait_send()
-        for level in range(across):
+    for shift in range(1, across):
+        slab_x(shift).wait_send()
+    for level in range(across):
+        for shift in range(1, broad):
+            slab_y(level, shift).wait_send()
+        for column in range(broad):
             slab_core(level, column).wait_send()
     for shift in range(1, count):
         remote_done(me, lax.rem(me + shift, count)).wait_send()
@@ -545,8 +558,8 @@
             sem((chunks, tall, 2)), sem((chunks, tall, beside)), sem((chunks, tall, across)),
             sem((chunks, tall, groups)),
             sem((chunks, broad, tall)), sem((chunks, count)),
-            sem((tall, 2)), sem((tall,)), sem((others,)), sem((broad,)),
-            sem((broad, beside)), sem((across, broad)), sem((across, broad)), sem((across, broad)),
+            sem((tall, 2)), sem((tall,)), sem((across, others)), sem((across, broad)),
+            sem((beside,)), sem((across,)), sem((across, broad)), sem((across, broad)),
             sem((count,)), sem((count,)),
         ],
         compiler_params=pltpu.CompilerParams(

time: 139 us -> 116 us (0.83)
  the two profiles are of different devices: /device:TPU:26 before, /device:TPU:29 now
where the time goes in v2:
time: 116 us
  Pallas kernels  114 us (98%)
  local copies, waits for them, and re-layouts  2.52 us (2%)
    pallas_call x1, Pallas kernels, on_device(): pl.pallas_call(functools.partial(layer_kernel, heads, width, count, group...  114 us
    unnamed x1, local copies, waits for them, and re-layouts  2.52 us

profile of v2, /device:TPU:29, one launch (start us, length us, event | category | flops | bytes accessed | tf_op | source)
XLA Modules:
  0.0 116.1 jit_solution(372393510799867930)
XLA Ops:
  0.0 113.6 %shard_map.73 = bf16[320,2048]{1,0:T(8,128)(2,1)} custom-call(bf16[320,2048]{1,0:T(8,128)(2,1)} %bitcast.4, bf16[512,128]{1,0:T(8,128)(2,1)} %wq_ref.1, bf16[512,128]{1,0:T(8,128)(2,1)} %wk_ref.1, bf16[512,128]{1,0:T(8,128)(2,1)} %wv_ref.1, bf16[128,512]{1,0:T(8,128)(2,1)} %slab_ref.1, f32[2,64]{1,0:T(2,128)} %gain_ref.1, f32[2,2560]{1,0:T(2,128)} %bitcast.5), custom_call_target="tpu_custom_call" | custom-call | tf_op jit(solution)/shard_map/pallas_call | solution.py:539
  113.6 2.5 %copy.9 = bf16[1,320,2048]{2,1,0:T(8,128)(2,1)} copy(bf16[1,320,2048]{2,1,0:T(8,128)(2,1)} %bitcast.3) | data formatting | bytes 2621440

commit v3 on v2

--- a/solution.py
+++ b/solution.py
@@ -21,17 +21,18 @@
 def layer_kernel(
     heads, width, count, groups,
     own_ref, wq_ref, wk_ref, wv_ref, slab_ref, gain_ref, decay_ref, out_ref,
-    far_ref, unit_weight_ref, value_weight_ref, slabs_ref, unit_stage_ref, value_stage_ref,
-    unit_ref, val_ref, key_ref, value_ref, done_ref, merged_ref,
+    far_ref, weight_ref, slabs_ref, stage_ref, full_ref, key_ref, value_ref, home_decay_ref,
+    near_stage_ref, near_ref, done_ref, merged_ref,
     far_send, far_recv, wz_send, wx_send, wc_send, w_recv, move_send, move_recv,
     sz_send, sz_recv, sy_send, sy_recv, sx_send, sx_recv, sc_send, sc_recv, done_send, done_recv,
+    near_send, near_recv, decay_send, decay_recv,
 ):
     rows, depth = own_ref.shape
     part = wq_ref.shape[0]
-    owners = 2
-    block = owners * rows
     wide = heads * width
     tall, broad, across = layout(count, groups)
+    block = broad * rows
+    span = wide + 16
     me, group = lax.axis_index("sp"), lax.axis_index("dp")
     z, y = me // broad, lax.rem(me, broad)
     x, core = group // CORES, lax.rem(group, CORES)
@@ -69,10 +70,8 @@
         for shift in range(1, broad)
     ]
 
-    chunks = [("unit", 0), ("value", 0)] + [("unit", head) for head in range(1, heads)]
-    weights = [
-        unit_weight_ref.at[head] if kind == "unit" else value_weight_ref for kind, head in chunks
-    ]
+    chunks = (wk_ref, wv_ref, wq_ref)
+    weights = [weight_ref.at[number] for number in range(3)]
 
     def weight(number, level, owner, out_sem, device):
         piece = weights[number].at[level, owner]
@@ -172,76 +171,81 @@
             for column in range(across):
                 to_core(number, level, column).wait_send()
 
-    lane = lax.broadcasted_iota(jnp.int32, (rows, 2 * width), 1)
-    gain = jnp.concatenate([gain_ref[0:1, :] * width ** (-0.5), gain_ref[1:2, :]], axis=1)
-
-    def unit(values):
+    def home_decay(turn):
+        place = pl.ds(pl.multiple_of(plane(turn) * block, block), block)
+        return remote(
+            decay_ref.at[:, place], home_decay_ref.at[z], decay_send.at[turn], decay_recv.at[z],
+            {"sp": plane(turn) * broad + y},
+        )
+
+    lane = lax.broadcasted_iota(jnp.int32, (rows, wide), 1)
+
+    def unit(values, gain):
         values = values.astype(jnp.bfloat16).astype(jnp.float32)
         squares = values * values
-        first = jnp.sum(jnp.where(lane < width, squares, 0.0), axis=-1, keepdims=True)
-        second = jnp.sum(jnp.where(lane < width, 0.0, squares), axis=-1, keepdims=True)
-        scale = jnp.where(
-            lane < width, lax.rsqrt(first / width + EPS), lax.rsqrt(second / width + EPS)
-        )
-        return values * scale * gain
+        scale = jnp.zeros_like(values)
+        for head in range(heads):
+            inside = (lane >= head * width) & (lane < (head + 1) * width)
+            total = jnp.sum(jnp.where(inside, squares, 0.0), axis=-1, keepdims=True)
+            scale = jnp.where(inside, lax.rsqrt(total / width + EPS), scale)
+        gains = jnp.concatenate([gain] * heads, axis=1)
+        return values * scale * gains
+
+    def row_place(source):
+        return pl.ds(pl.multiple_of(source * rows, rows), rows)
 
     def move(number, turn, side):
-        kind, head = chunks[number]
-        source = z * broad + along_y(side)
-        place = pl.ds(pl.multiple_of(source * rows, rows), rows)
-        if kind == "unit":
-            staged, target = unit_stage_ref.at[head, side, turn], unit_ref.at[head, place]
-        else:
-            staged, target = value_stage_ref.at[side, turn], val_ref.at[place]
+        column = along_y(side)
+        source = z * broad + column
         return remote(
-            staged, target, move_send.at[number, side, turn], move_recv.at[number, source],
+            stage_ref.at[number, turn, row_place(column)],
+            full_ref.at[number, row_place(source)],
+            move_send.at[number, side, turn], move_recv.at[number, source],
             {"sp": plane(turn) * broad + y},
         )
 
+    def needed(number, level):
+        return (level > 0) if number == 2 else (level < tall - 1)
+
     turns = sorted(range(tall), key=lambda turn: (turn == 0, turn != tall // 2))
 
     def project(number, side):
-        kind, head = chunks[number]
         values = own_ref[...] if side == 0 else far_ref[side - 1]
-        lanes = weights[number].shape[-1]
-        bunch = 2 if lanes % 128 == 0 and tall % 2 == 0 else 1
+        bunch = 2 if wide % 128 == 0 and tall % 2 == 0 else 1
         for first in range(0, tall, bunch):
             some = turns[first : first + bunch]
-            columns = [
-                weights[number][plane(turn)].reshape(depth, lanes) for turn in some
-            ]
+            columns = [weights[number][plane(turn)].reshape(depth, wide) for turn in some]
             result = jnp.dot(
                 values, columns[0] if bunch == 1 else jnp.concatenate(columns, axis=1),
                 preferred_element_type=jnp.float32,
             )
             for index, turn in enumerate(some):
-                piece = result[:, index * lanes : (index + 1) * lanes]
-                piece = (unit(piece) if kind == "unit" else piece).astype(jnp.bfloat16)
+                piece = result[:, index * wide : (index + 1) * wide]
+                if number == 0:
+                    piece = unit(piece, gain_ref[1:2, :])
+                elif number == 2:
+                    piece = unit(piece, gain_ref[0:1, :]) * width ** (-0.5)
+                piece = piece.astype(jnp.bfloat16)
+                stage_ref[number, turn, row_place(along_y(side)), :] = piece
+                if turn == 0:
+                    full_ref[number, row_place(z * broad + along_y(side)), :] = piece
+            for turn in some:
                 if turn:
-                    if kind == "unit":
-                        unit_stage_ref[head, side, turn] = piece
-                    else:
-                        value_stage_ref[side, turn] = piece
-                    move(number, turn, side).start()
-                else:
-                    place = (z * broad + along_y(side)) * rows
-                    place = pl.ds(pl.multiple_of(place, rows), rows)
-                    if kind == "unit":
-                        unit_ref[head, place, :] = piece
-                    else:
-                        val_ref[place, :] = piece
+                    @pl.when(needed(number, z))
+                    def _():
+                        move(number, turn, side).start()
 
     def moved(number):
-        kind, head = chunks[number]
         for turn in range(1, tall):
-            for column in range(broad):
-                source = plane(turn) * broad + column
-                place = pl.ds(pl.multiple_of(source * rows, rows), rows)
-                target = unit_ref.at[head, place] if kind == "unit" else val_ref.at[place]
-                remote(
-                    target, target, move_send.at[number, 0, turn], move_recv.at[number, source],
-                    {"sp": source},
-                ).wait_recv()
+            @pl.when(needed(number, plane(turn)))
+            def _():
+                for column in range(broad):
+                    source = plane(turn) * broad + column
+                    target = full_ref.at[number, row_place(source)]
+                    remote(
+                        target, target, move_send.at[number, 0, turn],
+                        move_recv.at[number, source], {"sp": source},
+                    ).wait_recv()
 
     tall_slab = slab_ref.shape[0]
 
@@ -327,13 +331,11 @@
                     {"dp": partner},
                 ).wait_recv()
 
-    for number, (kind, head) in enumerate(chunks):
-        if kind == "unit":
-            low = head * width
-            pair = [ref[:, low : low + width].astype(jnp.float32) for ref in (wq_ref, wk_ref)]
-            unit_weight_ref[head, z, group] = jnp.concatenate(pair, axis=1).astype(jnp.bfloat16)
-        else:
-            value_weight_ref[z, group] = wv_ref[...]
+    for turn in range(1, tall):
+        home_decay(turn).start()
+    home_decay_ref[z] = decay_ref[:, pl.ds(pl.multiple_of(z * block, block), block)]
+    for number in range(3):
+        weight_ref[number, z, group] = chunks[number][...]
         if number < 2:
             own_along_z(number)
             spread(number, z)
@@ -348,8 +350,7 @@
         relay_core(number)
         gathered(number)
 
-    last = len(chunks) - 1
-    rest = range(2, len(chunks))
+    rest = (2,)
     for distance in range(1, tall):
         relay(0, distance)
         if distance == 1:
@@ -385,60 +386,161 @@
             project(number, side)
     for distance in range(1, tall):
         slab_relay(distance)
-    slabs_of_y()
     for number in rest:
         ready(number)
         for side in range(broad):
             project(number, side)
-    for number in range(len(chunks)):
-        moved(number)
-
-    def remote_done(source, owner):
+
+    def split(values):
+        first = values.astype(jnp.bfloat16).astype(jnp.float32)
+        rest = values - first
+        second = rest.astype(jnp.bfloat16).astype(jnp.float32)
+        return first, second, rest - second
+
+    block_lane = lax.broadcasted_iota(jnp.int32, (block, 2 * width), 1)
+    ones_rows = jnp.where(lax.broadcasted_iota(jnp.int32, (16, block), 0) == 0, 1.0, 0.0)
+    packed = wide == 2 * width
+
+    def aside(head):
+        return width if packed and head == 0 else 0
+
+    def beside(head):
+        low = aside(head)
+        return (block_lane >= low) & (block_lane < low + width)
+
+    def with_lanes(values, head, lanes):
+        if packed:
+            return jnp.where(beside(head), lanes, values.astype(jnp.float32)).astype(jnp.bfloat16)
+        own = values[:, head * width : (head + 1) * width].astype(jnp.float32)
+        return jnp.concatenate([lanes[:, :width], own], axis=1).astype(jnp.bfloat16)
+
+    def query_operand(values, head):
+        low = aside(head)
+        ones = jnp.where((block_lane >= low) & (block_lane < low + 3), 1.0, 0.0)
+        return with_lanes(values, head, ones)
+
+    def key_operands(values, decay):
+        sub = lax.broadcasted_iota(jnp.int32, (2 * width, block), 0)
+        lanes = jnp.zeros((2 * width, block), jnp.float32)
+        fresh = []
+        for head in range(heads):
+            for index, piece in enumerate(split(-decay[head : head + 1, :])):
+                lanes = jnp.where(sub == aside(head) + index, piece, lanes)
+            if not packed:
+                fresh.append(with_lanes(values, head, lanes.T))
+        if packed:
+            turned = lanes.T
+            fresh = [with_lanes(values, head, turned) for head in range(heads)]
+        return fresh
+
+    def value_operands(values):
+        turned = values.astype(jnp.float32).T
+        return [
+            jnp.concatenate(
+                [turned[head * width : (head + 1) * width], ones_rows], axis=0
+            ).astype(jnp.bfloat16)
+            for head in range(heads)
+        ]
+
+    def finish(parts):
+        mixed, logs = [], []
+        for peak, total in parts:
+            norm = total[width : width + 1]
+            mixed.append(total[:width] / norm)
+            logs.extend(split(peak + jnp.log(norm)))
+        sub = lax.broadcasted_iota(jnp.int32, (16, block), 0)
+        tail = jnp.zeros((16, block), jnp.float32)
+        for index, piece in enumerate(logs):
+            tail = jnp.where(sub == index, piece, tail)
+        result = jnp.concatenate([*mixed, tail], axis=0)
+        return [
+            (pltpu.roll(result, block - column * rows, 1) if column else result)[
+                :, :rows
+            ].astype(jnp.bfloat16)
+            for column in range(broad)
+        ]
+
+    def scores_of(keys, queries):
+        return lax.dot_general(keys, queries, DIMS_NT, preferred_element_type=jnp.float32)
+
+    def near_copy(turn, side):
+        column = along_y(side)
         return remote(
-            done_ref.at[owner], merged_ref.at[source], done_send.at[owner], done_recv.at[source],
-            {"sp": owner},
-        )
-
-    def one_block(index, unused):
-        place = pl.ds(pl.multiple_of(index * block, block), block)
-        values_turned = val_ref[place, :].astype(jnp.float32).T
-        lane = lax.broadcasted_iota(jnp.int32, (block, 2 * width), 1)
-        ones_lanes = jnp.where(lane < 3, 1.0, 0.0)
-        sub = lax.broadcasted_iota(jnp.int32, (2 * width, block), 0)
-        ones_rows = jnp.where(
-            lax.broadcasted_iota(jnp.int32, (16, block), 0) == 0, 1.0, 0.0
-        )
-        queries = []
+            near_stage_ref.at[turn, column], near_ref.at[plane(turn) * broad + y],
+            near_send.at[turn, side], near_recv.at[plane(turn) * broad + y],
+            {"sp": z * broad + column},
+        )
+
+    key_place = lax.broadcasted_iota(jnp.int32, (block, block), 0)
+    query_place = lax.broadcasted_iota(jnp.int32, (block, block), 1)
+
+    def near_block(turn, unused):
+        keys = key_operands(stage_ref[0, turn], home_decay_ref[plane(turn)])
+        values = value_operands(stage_ref[1, turn])
+        parts = []
         for head in range(heads):
-            low = head * width
-            units = unit_ref[head, place, :].astype(jnp.float32)
-            decay = -decay_ref[head : head + 1, place]
-            first = decay.astype(jnp.bfloat16).astype(jnp.float32)
-            rest = decay - first
-            second = rest.astype(jnp.bfloat16).astype(jnp.float32)
-            third = rest - second
-            parts = jnp.where(
-                sub == 0, first, jnp.where(sub == 1, second, jnp.where(sub == 2, third, 0.0))
-            ).T
-            turned_units = pltpu.roll(units, width, 1)
-            queries.append(jnp.where(lane < width, ones_lanes, turned_units).astype(jnp.bfloat16))
-            key_ref[head, place, :] = jnp.where(lane < width, parts, units).astype(jnp.bfloat16)
-            value_ref[head, index] = jnp.concatenate(
-                [values_turned[low : low + width], ones_rows], axis=0
-            ).astype(jnp.bfloat16)
-
-        def step(column, carry, masked):
+            scores = scores_of(keys[head], query_operand(stage_ref[2, turn], head))
+            scores = jnp.where(key_place <= query_place, scores, -jnp.inf)
+            peak = jnp.max(scores, axis=0, keepdims=True)
+            probs = jnp.exp(scores - peak).astype(jnp.bfloat16)
+            parts.append(
+                (peak, jnp.dot(values[head], probs, preferred_element_type=jnp.float32))
+            )
+        for column, piece in enumerate(finish(parts)):
+            near_stage_ref[turn, column] = piece
+        near_ref[plane(turn) * broad + y] = near_stage_ref[turn, y]
+        for side in range(1, broad):
+            near_copy(turn, side).start()
+
+        @pl.when(turn == 0)
+        def _():
+            slabs_of_y()
+
+        @pl.when(turn == 2)
+        def _():
+            slabs_from_x()
+
+        return unused
+
+    for turn in range(1, tall):
+        remote(
+            home_decay_ref.at[plane(turn)], home_decay_ref.at[plane(turn)], decay_send.at[turn],
+            decay_recv.at[plane(turn)], {"sp": me},
+        ).wait_recv()
+    lax.fori_loop(0, tall, near_block, 0)
+
+    moved(0)
+    moved(1)
+
+    def prepare(level, unused):
+        place = pl.ds(pl.multiple_of(level * block, block), block)
+        keys = key_operands(full_ref[0, place, :], decay_ref[:, place])
+        values = value_operands(full_ref[1, place, :])
+        for head in range(heads):
+            key_ref[head, level] = keys[head]
+            value_ref[head, level] = values[head]
+        return unused
+
+    lax.fori_loop(0, tall - 1, prepare, 0)
+    moved(2)
+
+    def remote_done(level, column):
+        owner = level * broad + column
+        return remote(
+            done_ref.at[level, column], merged_ref.at[me], done_send.at[level, column],
+            done_recv.at[me], {"sp": owner},
+        )
+
+    def far_block(index, unused):
+        level = tall - 1 - index
+        place = pl.ds(pl.multiple_of(level * block, block), block)
+        queries = [query_operand(full_ref[2, place, :], head) for head in range(heads)]
+
+        def step(column, carry):
             fresh = []
             for head in range(heads):
                 peak, total = carry[head]
-                keys = key_ref[head, pl.ds(pl.multiple_of(column * block, block), block), :]
-                scores = lax.dot_general(
-                    keys, queries[head], DIMS_NT, preferred_element_type=jnp.float32
-                )
-                if masked:
-                    key_place = lax.broadcasted_iota(jnp.int32, scores.shape, 0)
-                    query_place = lax.broadcasted_iota(jnp.int32, scores.shape, 1)
-                    scores = jnp.where(key_place <= query_place, scores, -jnp.inf)
+                scores = scores_of(key_ref[head, column], queries[head])
                 higher = jnp.maximum(peak, jnp.max(scores, axis=0, keepdims=True))
                 probs = jnp.exp(scores - higher).astype(jnp.bfloat16)
                 total = total * jnp.exp(peak - higher) + jnp.dot(
@@ -454,41 +556,66 @@
             )
             for _ in range(heads)
         )
-        carry = step(index, start, True)
-        carry = lax.fori_loop(0, index, lambda column, c: step(column, c, False), carry)
+        carry = lax.fori_loop(0, level, step, start)
+        for column, piece in enumerate(finish(carry)):
+            done_ref[level, column] = piece
+
+            @pl.when(level * broad + column != me)
+            def _():
+                remote_done(level, column).start()
+
+        @pl.when(index == 0)
+        def _():
+            slabs_from_y()
+
+        return unused
+
+    lax.fori_loop(0, tall - 1, far_block, 0)
+
+    @pl.when(z > 0)
+    def _():
+        merged_ref[me] = done_ref[z, y]
+        for shift in range(1, count):
+            source = lax.rem(me + shift, count)
+            target = merged_ref.at[source]
+            remote(
+                target, target, done_send.at[0, 0], done_recv.at[source], {"sp": source}
+            ).wait_recv()
+
+    @pl.when(z == 0)
+    def _():
+        nothing = jnp.where(
+            lax.broadcasted_iota(jnp.int32, (span, rows), 0) < wide, 0.0, -1e30
+        ).astype(jnp.bfloat16)
+        for source in range(count):
+            merged_ref[source] = nothing
+
+    for turn in range(tall):
+        for side in range(1, broad):
+            target = near_ref.at[plane(turn) * broad + along_y(side)]
+            remote(
+                target, target, near_send.at[turn, side],
+                near_recv.at[plane(turn) * broad + along_y(side)], {"sp": me},
+            ).wait_recv()
+    slabs_from_core()
+
+    def combined(source):
+        one, two = (ref[source].astype(jnp.float32) for ref in (near_ref, merged_ref))
         outs = []
         for head in range(heads):
-            total = carry[head][1]
-            mixed, norm = total[:width], total[width : width + 1]
-            scale = lax.rsqrt(jnp.mean(mixed * mixed, axis=0, keepdims=True) + EPS * norm * norm)
+            low = wide + 3 * head
+            logs = [sum(part[low + i : low + i + 1] for i in range(3)) for part in (one, two)]
+            peak = jnp.maximum(*logs)
+            first, second = (jnp.exp(log - peak) for log in logs)
+            norm = first + second
+            place = slice(head * width, (head + 1) * width)
+            mixed = one[place] * (first / norm) + two[place] * (second / norm)
+            scale = lax.rsqrt(jnp.mean(mixed * mixed, axis=0, keepdims=True) + EPS)
             outs.append(mixed * scale)
-        turned = jnp.concatenate(outs, axis=0).T.astype(jnp.bfloat16)
-        for part_index in range(owners):
-            owner = index * owners + part_index
-            done_ref[owner] = turned[part_index * rows : (part_index + 1) * rows]
-
-            @pl.when(owner != me)
-            def _():
-                remote_done(me, owner).start()
-
-        @pl.when(index == 1)
-        def _():
-            slabs_from_x()
-
-        @pl.when(index == 3)
-        def _():
-            slabs_from_y()
-
-        return unused
-
-    lax.fori_loop(0, count // owners, one_block, 0)
-    merged_ref[me] = done_ref[me]
-    slabs_from_core()
-    for shift in range(1, count):
-        other = lax.rem(me + shift, count)
-        remote_done(other, other).wait_recv()
+        return jnp.concatenate(outs, axis=0).T.astype(jnp.bfloat16)
+
     merged = jnp.concatenate(
-        [merged_ref[level * broad + column] for column in range(broad) for level in range(tall)],
+        [combined(level * broad + column) for column in range(broad) for level in range(tall)],
         axis=1,
     )
     columns = slab_ref.shape[1]
@@ -499,11 +626,19 @@
 
     for copy in tokens:
         copy.wait_send()
-    for number in range(len(chunks)):
+    for number in range(3):
         weights_sent(number)
-        for side in range(broad):
-            for turn in range(1, tall):
-                move(number, turn, side).wait_send()
+
+        @pl.when(needed(number, z))
+        def _():
+            for side in range(broad):
+                for turn in range(1, tall):
+                    move(number, turn, side).wait_send()
+    for turn in range(tall):
+        if turn:
+            home_decay(turn).wait_send()
+        for side in range(1, broad):
+            near_copy(turn, side).wait_send()
     for distance in range(tall):
         for way in range(2):
             level = z - distance if way == 0 else z + distance
@@ -521,8 +656,11 @@
             slab_y(level, shift).wait_send()
         for column in range(broad):
             slab_core(level, column).wait_send()
-    for shift in range(1, count):
-        remote_done(me, lax.rem(me + shift, count)).wait_send()
+    for level in range(1, tall):
+        for column in range(broad):
+            @pl.when(level * broad + column != me)
+            def _():
+                remote_done(level, column).wait_send()
 
 
 def on_device(tokens, w_query, w_key, w_value, w_output, qk_gain, decay_sums):
@@ -532,9 +670,9 @@
     rows, depth = own_rows.shape
     part = w_query.shape[0]
     heads, width = decay_rows.shape[0], qk_gain.shape[1]
-    wide, length, block = heads * width, count * rows, 2 * rows
+    wide, length, block = heads * width, count * rows, broad * rows
     tall_slab, columns = w_output.shape
-    bf16, sem, chunks = jnp.bfloat16, pltpu.SemaphoreType.DMA, heads + 1
+    bf16, sem, span = jnp.bfloat16, pltpu.SemaphoreType.DMA, wide + 16
     others, beside = max(broad - 1, 1), max(across - 1, 1)
     result = pl.pallas_call(
         functools.partial(layer_kernel, heads, width, count, groups),
@@ -543,24 +681,25 @@
         out_specs=pl.BlockSpec(memory_space=pltpu.VMEM),
         scratch_shapes=[
             pltpu.VMEM((others, rows, depth), bf16),
-            pltpu.VMEM((heads, tall, groups, part, 2 * width), bf16),
-            pltpu.VMEM((tall, groups, part, wide), bf16),
+            pltpu.VMEM((3, tall, groups, part, wide), bf16),
             pltpu.VMEM((groups, broad, tall * tall_slab, columns), bf16),
-            pltpu.VMEM((heads, broad, tall, rows, 2 * width), bf16),
-            pltpu.VMEM((broad, tall, rows, wide), bf16),
-            pltpu.VMEM((heads, length, 2 * width), bf16),
-            pltpu.VMEM((length, wide), bf16),
-            pltpu.VMEM((heads, length, 2 * width), bf16),
-            pltpu.VMEM((heads, length // block, width + 16, block), bf16),
-            pltpu.VMEM((count, rows, wide), bf16),
-            pltpu.VMEM((count, rows, wide), bf16),
+            pltpu.VMEM((3, tall, block, wide), bf16),
+            pltpu.VMEM((3, length, wide), bf16),
+            pltpu.VMEM((heads, tall, block, 2 * width), bf16),
+            pltpu.VMEM((heads, tall, width + 16, block), bf16),
+            pltpu.VMEM((tall, heads, block), jnp.float32),
+            pltpu.VMEM((tall, broad, span, rows), bf16),
+            pltpu.VMEM((count, span, rows), bf16),
+            pltpu.VMEM((tall, broad, span, rows), bf16),
+            pltpu.VMEM((count, span, rows), bf16),
             sem((others,)), sem((others,)),
-            sem((chunks, tall, 2)), sem((chunks, tall, beside)), sem((chunks, tall, across)),
-            sem((chunks, tall, groups)),
-            sem((chunks, broad, tall)), sem((chunks, count)),
+            sem((3, tall, 2)), sem((3, tall, beside)), sem((3, tall, across)),
+            sem((3, tall, groups)),
+            sem((3, broad, tall)), sem((3, count)),
             sem((tall, 2)), sem((tall,)), sem((across, others)), sem((across, broad)),
             sem((beside,)), sem((across,)), sem((across, broad)), sem((across, broad)),
-            sem((count,)), sem((count,)),
+            sem((tall, broad)), sem((count,)),
+            sem((tall, broad)), sem((count,)), sem((tall,)), sem((tall,)),
         ],
         compiler_params=pltpu.CompilerParams(
             collective_id=0, has_side_effects=True, vmem_limit_bytes=60 * 1024 * 1024

time: 116 us -> 139 us (1.20)
  the two profiles are of different devices: /device:TPU:29 before, /device:TPU:12 now
where the time goes in v3:
time: 139 us
  Pallas kernels  136 us (98%)
  local copies, waits for them, and re-layouts  2.52 us (2%)
    pallas_call x1, Pallas kernels, on_device(): pl.pallas_call(functools.partial(layer_kernel, heads, width, count, group...  136 us

profile of v3, /device:TPU:12, one launch (start us, length us, event | category | flops | bytes accessed | tf_op | source)
XLA Modules:
  0.0 139.0 jit_solution(14834380479086702683)
XLA Ops:
  0.0 136.5 %shard_map.73 = bf16[320,2048]{1,0:T(8,128)(2,1)} custom-call(bf16[320,2048]{1,0:T(8,128)(2,1)} %bitcast.4, bf16[512,128]{1,0:T(8,128)(2,1)} %wq_ref.1, bf16[512,128]{1,0:T(8,128)(2,1)} %wk_ref.1, bf16[512,128]{1,0:T(8,128)(2,1)} %wv_ref.1, bf16[128,512]{1,0:T(8,128)(2,1)} %slab_ref.1, f32[2,64]{1,0:T(2,128)} %gain_ref.1, f32[2,2560]{1,0:T(2,128)} %bitcast.5), custom_call_target="tpu_custom_call" | custom-call | tf_op jit(solution)/shard_map/pallas_call | solution.py:677
  136.5 2.5 %copy.9 = bf16[1,320,2048]{2,1,0:T(8,128)(2,1)} copy(bf16[1,320,2048]{2,1,0:T(8,128)(2,1)} %bitcast.3) | data formatting | bytes 2621440

commit v4 on v3

--- a/solution.py
+++ b/solution.py
@@ -22,10 +22,10 @@
     heads, width, count, groups,
     own_ref, wq_ref, wk_ref, wv_ref, slab_ref, gain_ref, decay_ref, out_ref,
     far_ref, weight_ref, slabs_ref, stage_ref, full_ref, key_ref, value_ref, home_decay_ref,
-    near_stage_ref, near_ref, done_ref, merged_ref,
+    near_stage_ref, near_ref, done_ref, merged_ref, log_ref, logs_ref,
     far_send, far_recv, wz_send, wx_send, wc_send, w_recv, move_send, move_recv,
     sz_send, sz_recv, sy_send, sy_recv, sx_send, sx_recv, sc_send, sc_recv, done_send, done_recv,
-    near_send, near_recv, decay_send, decay_recv,
+    near_send, near_recv, decay_send, decay_recv, log_send, log_recv,
 ):
     rows, depth = own_ref.shape
     part = wq_ref.shape[0]
@@ -235,17 +235,16 @@
                     def _():
                         move(number, turn, side).start()
 
-    def moved(number):
-        for turn in range(1, tall):
-            @pl.when(needed(number, plane(turn)))
-            def _():
-                for column in range(broad):
-                    source = plane(turn) * broad + column
-                    target = full_ref.at[number, row_place(source)]
-                    remote(
-                        target, target, move_send.at[number, 0, turn],
-                        move_recv.at[number, source], {"sp": source},
-                    ).wait_recv()
+    def moved(number, level):
+        @pl.when((level != z) & needed(number, level))
+        def _():
+            for column in range(broad):
+                source = level * broad + column
+                target = full_ref.at[number, row_place(source)]
+                remote(
+                    target, target, move_send.at[number, 0, 0], move_recv.at[number, source],
+                    {"sp": source},
+                ).wait_recv()
 
     tall_slab = slab_ref.shape[0]
 
@@ -271,18 +270,18 @@
             def _():
                 slab_z(level, way).start()
 
-    def slab_x(shift):
+    def slab_y(shift):
         piece = slabs_ref.at[group, y]
         return remote(
-            piece, piece, sx_send.at[shift - 1], sx_recv.at[x],
+            piece, piece, sy_send.at[shift - 1], sy_recv.at[y],
+            {"sp": z * broad + along_y(shift)},
+        )
+
+    def slab_x(column, shift):
+        piece = slabs_ref.at[group, column]
+        return remote(
+            piece, piece, sx_send.at[column, shift - 1], sx_recv.at[x, column],
             {"dp": along_x(shift) * CORES + core},
-        )
-
-    def slab_y(level, shift):
-        piece = slabs_ref.at[level * CORES + core, y]
-        return remote(
-            piece, piece, sy_send.at[level, shift - 1], sy_recv.at[level, y],
-            {"sp": z * broad + along_y(shift)},
         )
 
     def slab_core(level, column):
@@ -291,34 +290,34 @@
             piece, piece, sc_send.at[level, column], sc_recv.at[level, column], {"dp": partner}
         )
 
-    def slab_spread(level):
+    def slab_spread(column):
+        for shift in range(1, across):
+            slab_x(column, shift).start()
+        slab_core(x, column).start()
+
+    def slabs_of_z():
         for shift in range(1, broad):
-            slab_y(level, shift).start()
-        slab_core(level, y).start()
-
-    def slabs_of_y():
-        for shift in range(1, across):
-            slab_x(shift).start()
-        slab_spread(x)
+            slab_y(shift).start()
+        slab_spread(y)
+
+    def slabs_from_y():
+        for shift in range(1, broad):
+            column = along_y(shift)
+            piece = slabs_ref.at[group, column]
+            remote(
+                piece, piece, sy_send.at[shift - 1], sy_recv.at[column], {"sp": me}
+            ).wait_recv()
+            slab_spread(column)
 
     def slabs_from_x():
-        for shift in range(1, across):
-            level = along_x(shift)
-            piece = slabs_ref.at[level * CORES + core, y]
-            remote(
-                piece, piece, sx_send.at[shift - 1], sx_recv.at[level], {"dp": group}
-            ).wait_recv()
-            slab_spread(level)
-
-    def slabs_from_y():
-        for turn in range(across):
-            level = along_x(turn)
-            for shift in range(1, broad):
-                column = along_y(shift)
+        for turn in range(broad):
+            column = along_y(turn)
+            for shift in range(1, across):
+                level = along_x(shift)
                 piece = slabs_ref.at[level * CORES + core, column]
                 remote(
-                    piece, piece, sy_send.at[level, shift - 1], sy_recv.at[level, column],
-                    {"sp": me},
+                    piece, piece, sx_send.at[column, shift - 1], sx_recv.at[level, column],
+                    {"dp": group},
                 ).wait_recv()
                 slab_core(level, column).start()
 
@@ -357,6 +356,7 @@
             relay(1, 1, across_too=False)
             for number in rest:
                 own_along_z(number)
+            slab_relay(0)
         elif distance == 2:
             relay(1, 1, onward=False)
             relay(1, 2, across_too=False)
@@ -364,6 +364,8 @@
         relay(number, 1, across_too=False)
     if tall > 2:
         relay(1, 2, onward=False)
+    if tall > 1:
+        slab_relay(1)
     ready(0)
     for distance in range(3, tall):
         relay(1, distance)
@@ -373,19 +375,21 @@
         relay(number, 1, onward=False)
         if tall > 2:
             relay(number, 2)
+    if tall > 2:
+        slab_relay(2)
     ready(1)
     for number in rest:
         for distance in range(3, tall):
             relay(number, distance)
     project(1, 0)
-    slab_relay(0)
     for copy in tokens:
         copy.wait_recv()
     for number in range(2):
         for side in range(1, broad):
             project(number, side)
-    for distance in range(1, tall):
+    for distance in range(3, tall):
         slab_relay(distance)
+    slabs_of_z()
     for number in rest:
         ready(number)
         for side in range(broad):
@@ -442,23 +446,26 @@
             for head in range(heads)
         ]
 
-    def finish(parts):
+    def averages(parts):
         mixed, logs = [], []
         for peak, total in parts:
             norm = total[width : width + 1]
             mixed.append(total[:width] / norm)
-            logs.extend(split(peak + jnp.log(norm)))
-        sub = lax.broadcasted_iota(jnp.int32, (16, block), 0)
-        tail = jnp.zeros((16, block), jnp.float32)
-        for index, piece in enumerate(logs):
-            tail = jnp.where(sub == index, piece, tail)
-        result = jnp.concatenate([*mixed, tail], axis=0)
+            logs.append(peak + jnp.log(norm))
+        return mixed, logs
+
+    def pieces(values):
         return [
-            (pltpu.roll(result, block - column * rows, 1) if column else result)[
-                :, :rows
-            ].astype(jnp.bfloat16)
+            (pltpu.roll(values, block - column * rows, 1) if column else values)[:, :rows]
             for column in range(broad)
         ]
+
+    def stacked(rows_of, extent):
+        sub = lax.broadcasted_iota(jnp.int32, (extent, block), 0)
+        result = jnp.zeros((extent, block), jnp.float32)
+        for index, piece in enumerate(rows_of):
+            result = jnp.where(sub == index, piece, result)
+        return result
 
     def scores_of(keys, queries):
         return lax.dot_general(keys, queries, DIMS_NT, preferred_element_type=jnp.float32)
@@ -486,19 +493,13 @@
             parts.append(
                 (peak, jnp.dot(values[head], probs, preferred_element_type=jnp.float32))
             )
-        for column, piece in enumerate(finish(parts)):
-            near_stage_ref[turn, column] = piece
+        mixed, logs = averages(parts)
+        tail = stacked([piece for log in logs for piece in split(log)], 16)
+        for column, piece in enumerate(pieces(jnp.concatenate([*mixed, tail], axis=0))):
+            near_stage_ref[turn, column] = piece.astype(jnp.bfloat16)
         near_ref[plane(turn) * broad + y] = near_stage_ref[turn, y]
         for side in range(1, broad):
             near_copy(turn, side).start()
-
-        @pl.when(turn == 0)
-        def _():
-            slabs_of_y()
-
-        @pl.when(turn == 2)
-        def _():
-            slabs_from_x()
 
         return unused
 
@@ -507,12 +508,12 @@
             home_decay_ref.at[plane(turn)], home_decay_ref.at[plane(turn)], decay_send.at[turn],
             decay_recv.at[plane(turn)], {"sp": me},
         ).wait_recv()
+    slabs_from_y()
     lax.fori_loop(0, tall, near_block, 0)
 
-    moved(0)
-    moved(1)
-
     def prepare(level, unused):
+        moved(0, level)
+        moved(1, level)
         place = pl.ds(pl.multiple_of(level * block, block), block)
         keys = key_operands(full_ref[0, place, :], decay_ref[:, place])
         values = value_operands(full_ref[1, place, :])
@@ -522,17 +523,23 @@
         return unused
 
     lax.fori_loop(0, tall - 1, prepare, 0)
-    moved(2)
 
     def remote_done(level, column):
-        owner = level * broad + column
-        return remote(
-            done_ref.at[level, column], merged_ref.at[me], done_send.at[level, column],
-            done_recv.at[me], {"sp": owner},
-        )
+        device = {"sp": level * broad + column}
+        return [
+            remote(
+                done_ref.at[level, column], merged_ref.at[me], done_send.at[level, column],
+                done_recv.at[me], device,
+            ),
+            remote(
+                log_ref.at[level, column], logs_ref.at[me], log_send.at[level, column],
+                log_recv.at[me], device,
+            ),
+        ]
 
     def far_block(index, unused):
         level = tall - 1 - index
+        moved(2, level)
         place = pl.ds(pl.multiple_of(level * block, block), block)
         queries = [query_operand(full_ref[2, place, :], head) for head in range(heads)]
 
@@ -557,16 +564,20 @@
             for _ in range(heads)
         )
         carry = lax.fori_loop(0, level, step, start)
-        for column, piece in enumerate(finish(carry)):
-            done_ref[level, column] = piece
+        mixed, logs = averages(carry)
+        turned = jnp.concatenate(mixed, axis=0).T.astype(jnp.bfloat16)
+        for column, piece in enumerate(pieces(stacked(logs, 8))):
+            log_ref[level, column] = piece
+            done_ref[level, column] = turned[column * rows : (column + 1) * rows]
 
             @pl.when(level * broad + column != me)
             def _():
-                remote_done(level, column).start()
-
-        @pl.when(index == 0)
+                for copy in remote_done(level, column):
+                    copy.start()
+
+        @pl.when(index == min(1, tall - 2))
         def _():
-            slabs_from_y()
+            slabs_from_x()
 
         return unused
 
@@ -575,20 +586,23 @@
     @pl.when(z > 0)
     def _():
         merged_ref[me] = done_ref[z, y]
+        logs_ref[me] = log_ref[z, y]
         for shift in range(1, count):
             source = lax.rem(me + shift, count)
-            target = merged_ref.at[source]
             remote(
-                target, target, done_send.at[0, 0], done_recv.at[source], {"sp": source}
+                merged_ref.at[source], merged_ref.at[source], done_send.at[0, 0],
+                done_recv.at[source], {"sp": source},
+            ).wait_recv()
+            remote(
+                logs_ref.at[source], logs_ref.at[source], log_send.at[0, 0],
+                log_recv.at[source], {"sp": source},
             ).wait_recv()
 
     @pl.when(z == 0)
     def _():
-        nothing = jnp.where(
-            lax.broadcasted_iota(jnp.int32, (span, rows), 0) < wide, 0.0, -1e30
-        ).astype(jnp.bfloat16)
         for source in range(count):
-            merged_ref[source] = nothing
+            merged_ref[source] = jnp.zeros((rows, wide), jnp.bfloat16)
+            logs_ref[source] = jnp.full((8, rows), -1e30, jnp.float32)
 
     for turn in range(tall):
         for side in range(1, broad):
@@ -600,11 +614,13 @@
     slabs_from_core()
 
     def combined(source):
-        one, two = (ref[source].astype(jnp.float32) for ref in (near_ref, merged_ref))
+        one = near_ref[source].astype(jnp.float32)
+        two = merged_ref[source].astype(jnp.float32).T
         outs = []
         for head in range(heads):
             low = wide + 3 * head
-            logs = [sum(part[low + i : low + i + 1] for i in range(3)) for part in (one, two)]
+            near_log = sum(one[low + i : low + i + 1] for i in range(3))
+            logs = near_log, logs_ref[source][head : head + 1]
             peak = jnp.maximum(*logs)
             first, second = (jnp.exp(log - peak) for log in logs)
             norm = first + second
@@ -649,18 +665,19 @@
             def _():
                 slab_z(level, way).wait_send()
 
-    for shift in range(1, across):
-        slab_x(shift).wait_send()
-    for level in range(across):
-        for shift in range(1, broad):
-            slab_y(level, shift).wait_send()
-        for column in range(broad):
+    for shift in range(1, broad):
+        slab_y(shift).wait_send()
+    for column in range(broad):
+        for shift in range(1, across):
+            slab_x(column, shift).wait_send()
+        for level in range(across):
             slab_core(level, column).wait_send()
     for level in range(1, tall):
         for column in range(broad):
             @pl.when(level * broad + column != me)
             def _():
-                remote_done(level, column).wait_send()
+                for copy in remote_done(level, column):
+                    copy.wait_send()
 
 
 def on_device(tokens, w_query, w_key, w_value, w_output, qk_gain, decay_sums):
@@ -690,16 +707,19 @@
             pltpu.VMEM((tall, heads, block), jnp.float32),
             pltpu.VMEM((tall, broad, span, rows), bf16),
             pltpu.VMEM((count, span, rows), bf16),
-            pltpu.VMEM((tall, broad, span, rows), bf16),
-            pltpu.VMEM((count, span, rows), bf16),
+            pltpu.VMEM((tall, broad, rows, wide), bf16),
+            pltpu.VMEM((count, rows, wide), bf16),
+            pltpu.VMEM((tall, broad, 8, rows), jnp.float32),
+            pltpu.VMEM((count, 8, rows), jnp.float32),
             sem((others,)), sem((others,)),
             sem((3, tall, 2)), sem((3, tall, beside)), sem((3, tall, across)),
             sem((3, tall, groups)),
             sem((3, broad, tall)), sem((3, count)),
-            sem((tall, 2)), sem((tall,)), sem((across, others)), sem((across, broad)),
-            sem((beside,)), sem((across,)), sem((across, broad)), sem((across, broad)),
+            sem((tall, 2)), sem((tall,)), sem((others,)), sem((broad,)),
+            sem((broad, beside)), sem((across, broad)), sem((across, broad)), sem((across, broad)),
             sem((tall, broad)), sem((count,)),
             sem((tall, broad)), sem((count,)), sem((tall,)), sem((tall,)),
+            sem((tall, broad)), sem((count,)),
         ],
         compiler_params=pltpu.CompilerParams(
             collective_id=0, has_side_effects=True, vmem_limit_bytes=60 * 1024 * 1024

time: 139 us -> 98.9 us (0.71)
  Pallas kernels: 136 us -> 96.2 us
    pallas_call x1, Pallas kernels: 136 us -> 96.2 us  [on_device(): pl.pallas_call(functools.partial(layer_kernel, heads, width, count, group...]
where the time goes in v4:
time: 98.9 us; the launch traced here: 98.8 us
  Pallas kernels  96.2 us (97%)
  local copies, waits for them, and re-layouts  2.52 us (3%)
    pallas_call x1, Pallas kernels, on_device(): pl.pallas_call(functools.partial(layer_kernel, heads, width, count, group...  96.2 us
    unnamed x1, local copies, waits for them, and re-layouts  2.52 us

profile of v4, /device:TPU:12, one launch (start us, length us, event | category | flops | bytes accessed | tf_op | source)
XLA Modules:
  0.0 98.8 jit_solution(13592027920033810234)
XLA Ops:
  0.0 96.2 %shard_map.73 = bf16[320,2048]{1,0:T(8,128)(2,1)} custom-call(bf16[320,2048]{1,0:T(8,128)(2,1)} %bitcast.4, bf16[512,128]{1,0:T(8,128)(2,1)} %wq_ref.1, bf16[512,128]{1,0:T(8,128)(2,1)} %wk_ref.1, bf16[512,128]{1,0:T(8,128)(2,1)} %wv_ref.1, bf16[128,512]{1,0:T(8,128)(2,1)} %slab_ref.1, f32[2,64]{1,0:T(2,128)} %gain_ref.1, f32[2,2560]{1,0:T(2,128)} %bitcast.5), custom_call_target="tpu_custom_call" | custom-call | tf_op jit(solution)/shard_map/pallas_call | solution.py:694
  96.3 2.5 %copy.9 = bf16[1,320,2048]{2,1,0:T(8,128)(2,1)} copy(bf16[1,320,2048]{2,1,0:T(8,128)(2,1)} %bitcast.3) | data formatting | bytes 2621440

commit v5 on v4

--- a/solution.py
+++ b/solution.py
@@ -295,10 +295,9 @@
             slab_x(column, shift).start()
         slab_core(x, column).start()
 
-    def slabs_of_z():
+    def slabs_of_z_along_y():
         for shift in range(1, broad):
             slab_y(shift).start()
-        slab_spread(y)
 
     def slabs_from_y():
         for shift in range(1, broad):
@@ -330,9 +329,6 @@
                     {"dp": partner},
                 ).wait_recv()
 
-    for turn in range(1, tall):
-        home_decay(turn).start()
-    home_decay_ref[z] = decay_ref[:, pl.ds(pl.multiple_of(z * block, block), block)]
     for number in range(3):
         weight_ref[number, z, group] = chunks[number][...]
         if number < 2:
@@ -341,27 +337,31 @@
         if number == 0:
             for copy in tokens:
                 copy.start()
-    slabs_ref[group, y, pl.ds(pl.multiple_of(z * tall_slab, tall_slab), tall_slab), :] = slab_ref[
-        ...
-    ]
+            slabs_ref[
+                group, y, pl.ds(pl.multiple_of(z * tall_slab, tall_slab), tall_slab), :
+            ] = slab_ref[...]
+    for turn in range(1, tall):
+        home_decay(turn).start()
+    home_decay_ref[z] = decay_ref[:, pl.ds(pl.multiple_of(z * block, block), block)]
 
     def ready(number):
         relay_core(number)
         gathered(number)
 
-    rest = (2,)
+    def steps(*distances):
+        return [distance for distance in distances if distance < tall]
+
     for distance in range(1, tall):
         relay(0, distance)
         if distance == 1:
             relay(1, 1, across_too=False)
-            for number in rest:
-                own_along_z(number)
+            own_along_z(2)
             slab_relay(0)
         elif distance == 2:
             relay(1, 1, onward=False)
             relay(1, 2, across_too=False)
-    for number in rest:
-        relay(number, 1, across_too=False)
+    if tall > 1:
+        relay(2, 1, across_too=False)
     if tall > 2:
         relay(1, 2, onward=False)
     if tall > 1:
@@ -370,17 +370,15 @@
     for distance in range(3, tall):
         relay(1, distance)
     project(0, 0)
-    for number in rest:
-        spread(number, z)
-        relay(number, 1, onward=False)
-        if tall > 2:
-            relay(number, 2)
+    spread(2, z)
+    if tall > 1:
+        relay(2, 1, onward=False)
     if tall > 2:
+        relay(2, 2)
         slab_relay(2)
     ready(1)
-    for number in rest:
-        for distance in range(3, tall):
-            relay(number, distance)
+    for distance in range(3, tall):
+        relay(2, distance)
     project(1, 0)
     for copy in tokens:
         copy.wait_recv()
@@ -389,11 +387,11 @@
             project(number, side)
     for distance in range(3, tall):
         slab_relay(distance)
-    slabs_of_z()
-    for number in rest:
-        ready(number)
-        for side in range(broad):
-            project(number, side)
+    slabs_of_z_along_y()
+    slab_spread(y)
+    ready(2)
+    for side in range(broad):
+        project(2, side)
 
     def split(values):
         first = values.astype(jnp.bfloat16).astype(jnp.float32)
@@ -469,6 +467,16 @@
 
     def scores_of(keys, queries):
         return lax.dot_general(keys, queries, DIMS_NT, preferred_element_type=jnp.float32)
+
+    def online(carry, keys, queries, values):
+        peak, total = carry
+        scores = scores_of(keys, queries)
+        higher = jnp.maximum(peak, jnp.max(scores, axis=0, keepdims=True))
+        probs = jnp.exp(scores - higher).astype(jnp.bfloat16)
+        total = total * jnp.exp(peak - higher) + jnp.dot(
+            values, probs, preferred_element_type=jnp.float32
+        )
+        return higher, total
 
     def near_copy(turn, side):
         column = along_y(side)
@@ -511,7 +519,7 @@
     slabs_from_y()
     lax.fori_loop(0, tall, near_block, 0)
 
-    def prepare(level, unused):
+    def prepare(level):
         moved(0, level)
         moved(1, level)
         place = pl.ds(pl.multiple_of(level * block, block), block)
@@ -520,9 +528,6 @@
         for head in range(heads):
             key_ref[head, level] = keys[head]
             value_ref[head, level] = values[head]
-        return unused
-
-    lax.fori_loop(0, tall - 1, prepare, 0)
 
     def remote_done(level, column):
         device = {"sp": level * broad + column}
@@ -538,23 +543,21 @@
         ]
 
     def far_block(index, unused):
-        level = tall - 1 - index
+        level = lax.rem(index + 1, max(tall - 1, 1)) + 1
+        for column in range(tall - 1):
+            @pl.when(index == max(column - 1, 0))
+            def _():
+                prepare(column)
+
         moved(2, level)
         place = pl.ds(pl.multiple_of(level * block, block), block)
         queries = [query_operand(full_ref[2, place, :], head) for head in range(heads)]
 
         def step(column, carry):
-            fresh = []
-            for head in range(heads):
-                peak, total = carry[head]
-                scores = scores_of(key_ref[head, column], queries[head])
-                higher = jnp.maximum(peak, jnp.max(scores, axis=0, keepdims=True))
-                probs = jnp.exp(scores - higher).astype(jnp.bfloat16)
-                total = total * jnp.exp(peak - higher) + jnp.dot(
-                    value_ref[head, column], probs, preferred_element_type=jnp.float32
-                )
-                fresh.append((higher, total))
-            return tuple(fresh)
+            return tuple(
+                online(carry[head], key_ref[head, column], queries[head], value_ref[head, column])
+                for head in range(heads)
+            )
 
         start = tuple(
             (

time: 98.9 us -> 95.9 us (0.970)
  Pallas kernels: 96.2 us -> 93.2 us
    pallas_call x1, Pallas kernels: 96.2 us -> 93.2 us  [on_device(): pl.pallas_call(functools.partial(layer_kernel, heads, width, count, group...]
where the time goes in v5:
time: 95.9 us; the launch traced here: 95.7 us
  Pallas kernels  93.2 us (97%)
  local copies, waits for them, and re-layouts  2.52 us (3%)
    pallas_call x1, Pallas kernels, on_device(): pl.pallas_call(functools.partial(layer_kernel, heads, width, count, group...  93.2 us
    unnamed x1, local copies, waits for them, and re-layouts  2.52 us

profile of v5, /device:TPU:12, one launch (start us, length us, event | category | flops | bytes accessed | tf_op | source)
XLA Modules:
  0.0 95.7 jit_solution(13656694083370552942)
XLA Ops:
  0.0 93.2 %shard_map.73 = bf16[320,2048]{1,0:T(8,128)(2,1)} custom-call(bf16[320,2048]{1,0:T(8,128)(2,1)} %bitcast.4, bf16[512,128]{1,0:T(8,128)(2,1)} %wq_ref.1, bf16[512,128]{1,0:T(8,128)(2,1)} %wk_ref.1, bf16[512,128]{1,0:T(8,128)(2,1)} %wv_ref.1, bf16[128,512]{1,0:T(8,128)(2,1)} %slab_ref.1, f32[2,64]{1,0:T(2,128)} %gain_ref.1, f32[2,2560]{1,0:T(2,128)} %bitcast.5), custom_call_target="tpu_custom_call" | custom-call | tf_op jit(solution)/shard_map/pallas_call | solution.py:697
  93.2 2.5 %copy.9 = bf16[1,320,2048]{2,1,0:T(8,128)(2,1)} copy(bf16[1,320,2048]{2,1,0:T(8,128)(2,1)} %bitcast.3) | data formatting | bytes 2621440

commit v6 on v5

--- a/solution.py
+++ b/solution.py
@@ -543,10 +543,9 @@
         ]
 
     def far_block(index, unused):
-        level = lax.rem(index + 1, max(tall - 1, 1)) + 1
+        level = (index + 1) % max(tall - 1, 1) + 1
         for column in range(tall - 1):
-            @pl.when(index == max(column - 1, 0))
-            def _():
+            if index == max(column - 1, 0):
                 prepare(column)
 
         moved(2, level)
@@ -566,7 +565,9 @@
             )
             for _ in range(heads)
         )
-        carry = lax.fori_loop(0, level, step, start)
+        carry = start
+        for column in range(level):
+            carry = step(column, carry)
         mixed, logs = averages(carry)
         turned = jnp.concatenate(mixed, axis=0).T.astype(jnp.bfloat16)
         for column, piece in enumerate(pieces(stacked(logs, 8))):
@@ -578,13 +579,13 @@
                 for copy in remote_done(level, column):
                     copy.start()
 
-        @pl.when(index == min(1, tall - 2))
-        def _():
+        if index == min(1, tall - 2):
             slabs_from_x()
 
         return unused
 
-    lax.fori_loop(0, tall - 1, far_block, 0)
+    for index in range(tall - 1):
+        far_block(index, 0)
 
     @pl.when(z > 0)
     def _():

time: 95.9 us -> 94.5 us (0.985)
  Pallas kernels: 93.2 us -> 91.8 us
    pallas_call x1, Pallas kernels: 93.2 us -> 91.8 us  [on_device(): pl.pallas_call(functools.partial(layer_kernel, heads, width, count, group...]
where the time goes in v6:
time: 94.5 us; the launch traced here: 94.4 us
  Pallas kernels  91.8 us (97%)
  local copies, waits for them, and re-layouts  2.52 us (3%)
    pallas_call x1, Pallas kernels, on_device(): pl.pallas_call(functools.partial(layer_kernel, heads, width, count, group...  91.8 us
    unnamed x1, local copies, waits for them, and re-layouts  2.52 us

profile of v6, /device:TPU:12, one launch (start us, length us, event | category | flops | bytes accessed | tf_op | source)
XLA Modules:
  0.0 94.4 jit_solution(7228282746210335163)
XLA Ops:
  0.0 91.8 %shard_map.73 = bf16[320,2048]{1,0:T(8,128)(2,1)} custom-call(bf16[320,2048]{1,0:T(8,128)(2,1)} %bitcast.4, bf16[512,128]{1,0:T(8,128)(2,1)} %wq_ref.1, bf16[512,128]{1,0:T(8,128)(2,1)} %wk_ref.1, bf16[512,128]{1,0:T(8,128)(2,1)} %wv_ref.1, bf16[128,512]{1,0:T(8,128)(2,1)} %slab_ref.1, f32[2,64]{1,0:T(2,128)} %gain_ref.1, f32[2,2560]{1,0:T(2,128)} %bitcast.5), custom_call_target="tpu_custom_call" | custom-call | tf_op jit(solution)/shard_map/pallas_call | solution.py:698
  91.8 2.5 %copy.9 = bf16[1,320,2048]{2,1,0:T(8,128)(2,1)} copy(bf16[1,320,2048]{2,1,0:T(8,128)(2,1)} %bitcast.3) | data formatting | bytes 2621440
